TPU v7x, 32 devices: a whole 2x2x4 slice. The times are simulated.
32 devices in a mesh: sp: 8 (over z, y), tp: 4 (over x, core).
Axes of the slice: x: 2, y: 2, z: 4, core: 2. Of those that a mesh axis runs over, the one named last changes fastest.
Arguments:
- tokens: bfloat16 [6144, 2048], P(('sp', 'tp')), may hold values from -6 to 6
- norm_gain: float32 [2048], replicated, may hold values from 0.1 to 1.9
- w_query: bfloat16 [2048, 1024], P('sp', 'tp'), may hold values from -0.125 to 0.125
- w_forget: bfloat16 [2048, 1024], P('sp', 'tp'), may hold values from -0.125 to 0.125
- w_input: bfloat16 [2048, 1024], P('sp', 'tp'), may hold values from -0.125 to 0.125
- w_outgate: bfloat16 [2048, 1024], P('sp', 'tp'), may hold values from -0.125 to 0.125
- w_conv_value: bfloat16 [2048, 1024], P('sp', 'tp'), may hold values from -0.125 to 0.125
- w_conv_gate: bfloat16 [2048, 1024], P('sp', 'tp'), may hold values from -0.125 to 0.125
- w_gate_rec: bfloat16 [2048, 2048], P('sp', 'tp'), may hold values from -0.125 to 0.125
- w_gate_conv: bfloat16 [2048, 2048], P('sp', 'tp'), may hold values from -0.125 to 0.125
- lower_bound: float32 [1024], P('tp'), may hold values from 0.92 to 0.99991862, as said below
- decay_shift: float32 [6144, 1024], P('sp', 'tp'), may hold values from -0.7 to 0, as said below
- state_init: float32 [8, 128, 128], P('tp'), may hold values from -0.1875 to 0.1875
- head_gain: float32 [1024], P('tp'), may hold values from 0.1 to 1.9
- conv_kernel: float32 [31, 1024], P(None, 'tp'), may hold values from -7.5 to 7.5
- channel_gain: float32 [1024], P('tp'), may hold values from 0.1 to 1.9
- channel_bias: float32 [1024], P('tp'), may hold values from -3 to 3
- w_out_rec: bfloat16 [1024, 2048], P('tp', 'sp'), may hold values from -0.1875 to 0.1875
- w_out_conv: bfloat16 [1024, 2048], P('tp', 'sp'), may hold values from -0.1875 to 0.1875
Outputs:
- mixed_out: bfloat16 [6144, 2048], P('sp', 'tp')
Inputs may be any that keep to these rules, and one draw needn't show every extreme that they name: `lower_bound`: every entry is below one. `decay_shift`: no entry is positive.
All inputs are finite; a program needn't handle non-finite values.
Results may differ from a plain program's by a relative error of at most 0.017.
Values may be sent and summed in bfloat16 or wider, within the bound.
A program may use at most 64 MiB of HBM per device.

v0:
```python
import jax
import jax.numpy as jnp
from jax import lax
from jax.sharding import PartitionSpec as P

HEAD = 128
CONV = 1024
KW = 31
BLOCK = 64


EPSILON = 1e-06
highest_precision = lax.Precision.HIGHEST


def prefix(array, axis, combine, identity):
    size, position = (lax.axis_size(axis), lax.axis_index(axis))
    everything = jax.tree.map(
        lambda part, kind: lax.all_gather(part.astype(kind), axis),
        array,
        (jnp.bfloat16, jnp.bfloat16),
    )
    start = jax.tree.map(
        lambda part, zero: jnp.broadcast_to(jnp.asarray(zero, part.dtype), part.shape),
        array,
        identity,
    )

    def lap(k, before):
        reached = k < position
        new = combine(
            before, jax.tree.map(lambda part, own: part[k].astype(own.dtype), everything, array)
        )
        return jax.tree.map(lambda a, b: jnp.where(reached, a, b), new, before)

    return lax.fori_loop(0, size, lap, start)


def passed_along(block, axis, distance):
    devices = range(lax.axis_size(axis))
    route = [(i - distance, i) for i in devices if i - distance in devices]
    return lax.ppermute(block, axis, route)


def normalize_rows(values, gain_vector):
    widened = values.astype(jnp.float32)
    scale = lax.rsqrt(jnp.mean(widened * widened, axis=-1, keepdims=True) + EPSILON)
    return (widened * scale * gain_vector).astype(jnp.bfloat16)


def block_step(state, inputs):
    query, input_gate, values, log_decay = inputs
    length = query.shape[1]
    causal_masked = (jnp.arange(length)[:, None] >= jnp.arange(length)[None, :])[None, :, :, None]
    cumulative = jnp.cumsum(log_decay, axis=1)
    spread = cumulative[:, :, None, :] - cumulative[:, None, :, :]
    weight = jnp.where(causal_masked, jnp.exp(jnp.where(causal_masked, spread, 0.0)), 0.0)
    scores = jnp.einsum("htd,hsd,htsd->hts", query, input_gate, weight, precision=highest_precision)
    output = jnp.einsum("hts,hsv->htv", scores, values, precision=highest_precision)
    output = output + jnp.einsum(
        "htd,hdv->htv", query * jnp.exp(cumulative), state, precision=highest_precision
    )
    final = cumulative[:, -1:, :]
    carried = jnp.exp(final[:, 0, :])[:, :, None] * state
    carried = carried + jnp.einsum(
        "hsd,hsv->hdv",
        input_gate * jnp.exp(final - cumulative),
        values,
        precision=highest_precision,
    )
    return (carried, output)


def compose(preceding_segment, later):
    return (preceding_segment[0] * later[0], later[0][..., None] * preceding_segment[1] + later[1])


def local(
    tokens,
    norm_gain,
    w_query,
    w_forget,
    w_input,
    w_outgate,
    w_conv_value,
    w_conv_gate,
    w_gate_rec,
    w_gate_conv,
    lower_bound,
    decay_shift,
    state_init,
    head_gain,
    conv_kernel,
    channel_gain,
    channel_bias,
    w_out_rec,
    w_out_conv,
):
    tp_count = lax.axis_size("tp")
    normed = normalize_rows(lax.all_gather(tokens, "tp", axis=0, tiled=True), norm_gain)
    row_count = normed.shape[0]
    weights = (
        w_query,
        w_forget,
        w_input,
        w_outgate,
        w_conv_value,
        w_conv_gate,
        w_gate_rec,
        w_gate_conv,
    )
    portions = (
        lax.all_gather(weights[0], "sp", axis=0, tiled=True),
        lax.all_gather(weights[1], "sp", axis=0, tiled=True),
        lax.all_gather(weights[2], "sp", axis=0, tiled=True),
        lax.all_gather(weights[3], "sp", axis=0, tiled=True),
        lax.all_gather(weights[4], "sp", axis=0, tiled=True),
        lax.all_gather(weights[5], "sp", axis=0, tiled=True),
        lax.all_gather(weights[6], "sp", axis=0, tiled=True),
        lax.all_gather(weights[7], "sp", axis=0, tiled=True),
    )
    sums = tuple(
        (jnp.dot(normed, portion, preferred_element_type=jnp.float32) for portion in portions)
    )
    (
        query_raw,
        forget_raw,
        input_raw,
        outgate_raw,
        value_raw,
        gate_raw,
        gate_rec_raw,
        gate_conv_raw,
    ) = tuple((overall_aggregate.astype(jnp.bfloat16) for overall_aggregate in sums))
    local_heads = w_query.shape[1] // HEAD
    block_count = row_count // BLOCK
    query = jax.nn.silu(query_raw.astype(jnp.float32))
    input_gate = (1.0 - lower_bound) * jax.nn.sigmoid(-forget_raw.astype(jnp.float32))
    log_decay = jnp.log1p(-input_gate) + decay_shift
    values = input_raw.astype(jnp.float32)

    def to_blocks(array):
        return array.reshape(block_count, BLOCK, local_heads, HEAD).transpose(0, 2, 1, 3)

    zero_state = jnp.zeros((local_heads, HEAD, HEAD), jnp.float32)
    local_state, blocks_out = lax.scan(
        block_step,
        zero_state,
        (to_blocks(query), to_blocks(input_gate), to_blocks(values), to_blocks(log_decay)),
    )
    local_out = blocks_out.transpose(0, 2, 1, 3).reshape(row_count, local_heads, HEAD)
    running = jnp.cumsum(log_decay, axis=0)
    cumulated_forgetting = jnp.exp(running[-1]).reshape(local_heads, HEAD)
    ones_decay = jnp.ones_like(cumulated_forgetting)
    prefix_decay, prefix_state = prefix(
        (cumulated_forgetting, local_state), "sp", compose, (ones_decay, zero_state)
    )
    incoming_state = prefix_decay[:, :, None] * state_init + prefix_state
    decayed_query = (query * jnp.exp(running)).reshape(row_count, local_heads, HEAD)
    head_out = local_out + jnp.einsum(
        "thd,hdv->thv", decayed_query, incoming_state, precision=highest_precision
    )
    head_out = head_out * lax.rsqrt(jnp.mean(head_out * head_out, axis=-1, keepdims=True) + EPSILON)
    head_out = head_out * head_gain.reshape(local_heads, HEAD)
    mixed_rec = (
        head_out.reshape(row_count, local_heads * HEAD)
        * jax.nn.silu(outgate_raw.astype(jnp.float32))
    ).astype(jnp.bfloat16)
    gated = (value_raw.astype(jnp.float32) * jax.nn.sigmoid(gate_raw.astype(jnp.float32))).astype(
        jnp.bfloat16
    )
    rim_width = KW - 1
    previous = passed_along(gated[row_count - rim_width :], "sp", 1)
    extended = jnp.concatenate([previous, gated], axis=0).astype(jnp.float32)
    conv_out = jnp.zeros((row_count, gated.shape[1]), jnp.float32)
    for tap_index in range(KW):
        conv_out = conv_out + conv_kernel[tap_index] * extended[tap_index : tap_index + row_count]
    squares = lax.psum(jnp.sum(conv_out * conv_out, axis=1), "tp")
    scale = lax.rsqrt(squares / CONV + EPSILON)[:, None]
    mixed_conv = jax.nn.silu(conv_out * scale * channel_gain + channel_bias).astype(jnp.bfloat16)
    rec_columns, conv_columns = (
        lax.all_gather(w_out_rec, "sp", axis=1, tiled=True),
        lax.all_gather(w_out_conv, "sp", axis=1, tiled=True),
    )
    rec_width = mixed_rec.shape[1]
    rec_whole, conv_whole = (
        lax.all_gather(rec_columns, "tp", axis=0, tiled=True),
        lax.all_gather(conv_columns, "tp", axis=0, tiled=True),
    )
    both = jnp.concatenate([mixed_rec, mixed_conv], axis=1).reshape(
        tp_count, row_count // tp_count, -1
    )
    arrived = lax.all_to_all(both, "tp", split_axis=0, concat_axis=2, tiled=True)
    item_count = arrived.shape[1]
    grouped = arrived.reshape(item_count, tp_count, -1)
    rec_part = grouped[:, :, :rec_width].reshape(item_count, -1)
    conv_part = grouped[:, :, rec_width:].reshape(item_count, -1)
    first = jnp.dot(rec_part, rec_whole, preferred_element_type=jnp.float32).astype(jnp.bfloat16)
    second = jnp.dot(conv_part, conv_whole, preferred_element_type=jnp.float32).astype(jnp.bfloat16)
    projected = jnp.stack([first, second], axis=1)[None]
    returned = lax.all_to_all(projected[0], "tp", split_axis=2, concat_axis=0, tiled=True)
    y_rec = returned[:, 0]
    y_conv = returned[:, 1]
    merged = jax.nn.sigmoid(gate_rec_raw.astype(jnp.float32)) * y_rec.astype(jnp.float32)
    merged = merged + jax.nn.sigmoid(gate_conv_raw.astype(jnp.float32)) * y_conv.astype(jnp.float32)
    return merged.astype(jnp.bfloat16)


def solution(mesh):
    in_specs = (
        P(("sp", "tp"), None),
        P(),
        P("sp", "tp"),
        P("sp", "tp"),
        P("sp", "tp"),
        P("sp", "tp"),
        P("sp", "tp"),
        P("sp", "tp"),
        P("sp", "tp"),
        P("sp", "tp"),
        P("tp"),
        P("sp", "tp"),
        P("tp", None, None),
        P("tp"),
        P(None, "tp"),
        P("tp"),
        P("tp"),
        P("tp", "sp"),
        P("tp", "sp"),
    )
    out_specs = P("sp", "tp")
    return jax.shard_map(local, mesh=mesh, in_specs=in_specs, out_specs=out_specs, check_vma=False)
```

profile of v0, /device:TPU:0, one launch (start us, length us, event | category | flops | bytes accessed | tf_op | source)
XLA Modules:
  0.0 553.2 jit_solution(8562246545925976769)
XLA Ops:
  12.8 38.8 %all-gather.31.cloned.1.call-done = bf16[256,2048]{1,0:T(8,128)(2,1)} async-done(((bf16[256,256]{1,0:T(8,128)(2,1)}), bf16[256,2048]{1,0:T(8,128)(2,1)}) %all-gather.31.cloned.1.call-update) | async-done | bytes 1048592 | tf_op jit(solution)/shard_map/all_gather | solution.py:182
  51.6 40.4 %all-gather.35.cloned.1.call-done = bf16[256,2048]{1,0:T(8,128)(2,1)} async-done(((bf16[256,256]{1,0:T(8,128)(2,1)}), bf16[256,2048]{1,0:T(8,128)(2,1)}) %all-gather.35.cloned.1.call-update) | async-done | bytes 1048592 | tf_op jit(solution)/shard_map/all_gather | solution.py:183
  94.8 26.4 %all-gather.15.cloned.1.call-done = bf16[768,2048]{1,0:T(8,128)(2,1)} async-done(((bf16[192,2048]{1,0:T(8,128)(2,1)}), bf16[768,2048]{1,0:T(8,128)(2,1)}) %all-gather.15.cloned.1.call-update) | async-done | bytes 3145744 | tf_op jit(solution)/shard_map/all_gather | solution.py:100
  126.4 37.0 %all-gather.19.cloned.1.call-done = bf16[2048,256]{1,0:T(8,128)(2,1)} async-done(((bf16[256,256]{1,0:T(8,128)(2,1)}), bf16[2048,256]{1,0:T(8,128)(2,1)}) %all-gather.19.cloned.1.call-update) | async-done | bytes 1048592 | tf_op jit(solution)/shard_map/all_gather | solution.py:114
  167.7 36.7 %all-gather.23.cloned.1.call-done = bf16[2048,256]{1,0:T(8,128)(2,1)} async-done(((bf16[256,256]{1,0:T(8,128)(2,1)}), bf16[2048,256]{1,0:T(8,128)(2,1)}) %all-gather.23.cloned.1.call-update) | async-done | bytes 1048592 | tf_op jit(solution)/shard_map/all_gather | solution.py:113
  208.9 36.6 %all-gather.21.cloned.1.call-done = bf16[2048,256]{1,0:T(8,128)(2,1)} async-done(((bf16[256,256]{1,0:T(8,128)(2,1)}), bf16[2048,256]{1,0:T(8,128)(2,1)}) %all-gather.21.cloned.1.call-update) | async-done | bytes 1048592 | tf_op jit(solution)/shard_map/all_gather | solution.py:115
  245.4 4.1 fusion.40
  255.0 115.7 %while.29 = (s32[]{:T(128)}, f32[2,128,128]{2,1,0:T(8,128)S(1)}, f32[12,2,64,128]{3,2,0,1:T(8,128)}, f32[12,2,64,128]{3,2,1,0:T(8,128)}, f32[12,2,64,128]{3,2,1,...) while((s32[]{:T(128)}, f32[2,128,128]{2,1,0:T(8,128)S(1)}, ...), condition=%wide.region_3.4_spmd.clone, body=%wide.region_1.3_spmd.clone.sunk | while | flops 70430720 | bytes 10207360 | solution.py:146
  257.8 3.5 fusion.121
  306.0 3.5 fusion.121
  344.6 3.5 fusion.121
  370.7 31.6 %all-gather = bf16[16,128,128]{2,1,0:T(8,128)(2,1)S(1)} all-gather(bf16[2,128,128]{2,1,0:T(8,128)(2,1)S(1)} %convert_element_type.138), channel_id=2, replica_groups=mesh['sp'=8,'tp'=4] {'sp'}, dimensions={0}, use_global_device_ids=true | all-gather | bytes 589824 | tf_op jit(solution)/shard_map/all_gather | solution.py:19
  403.5 18.4 %all_gather.54 = bf16[8,2,128]{2,1,0:T(2,128)(2,1)S(1)} all-gather(bf16[1,2,128]{2,1,0:T(2,128)(2,1)S(1)} %bitcast.230), channel_id=1, replica_groups=mesh['sp'=8,'tp'=4] {'sp'}, dimensions={0}, use_global_device_ids=true | all-gather | bytes 4608 | tf_op jit(solution)/shard_map/all_gather | solution.py:19
  427.2 4.2 fusion.37
  443.5 5.7 %psum.7 = f32[768]{0:T(1024)S(1)} all-reduce(f32[768]{0:T(1024)S(1)} %get-tuple-element.228), channel_id=1, replica_groups=mesh['sp'=8,'tp'=4] {'tp'}, use_global_device_ids=true, to_apply=%region_10.11 | all-reduce | flops 768 | bytes 6144 | tf_op jit(solution)/shard_map/psum | solution.py:178
  449.6 14.1 %all_to_all.33 = bf16[4,192,512]{2,1,0:T(8,128)(2,1)S(1)} all-to-all(bf16[4,192,512]{2,1,0:T(8,128)(2,1)S(1)} %bitcast.188), channel_id=1, replica_groups=mesh['sp'=8,'tp'=4] {'tp'}, dimensions={0} | all-to-all | bytes 1572864 | tf_op jit(solution)/shard_map/all_to_all | solution.py:193
  470.6 3.8 copy.86
  474.5 3.8 all-to-all-start.1
  478.3 12.4 %all-gather.39.cloned.1.call-done = bf16[2048,512]{1,0:T(8,128)(2,1)} async-done(((bf16[256,512]{1,0:T(8,128)(2,1)}), bf16[2048,512]{1,0:T(8,128)(2,1)}) %all-gather.39.cloned.1.call-update) | async-done | bytes 2097168 | tf_op jit(solution)/shard_map/all_gather | solution.py:120
  490.7 4.3 convolution_convert_fusion.2
  495.0 8.7 %all-to-all-done.1 = bf16[192,2,2048]{0,1,2:T(2,128)(2,1)S(1)} async-done(((bf16[192,2,2048]{0,1,2:T(2,128)(2,1)}), bf16[192,2,2048]{0,1,2:T(2,128)(2,1)S(1)}, u32[]{:S(2)}, u32[]{:S(2)}) %all-to-all-start.1) | async-done | bytes 1572896 | tf_op jit(solution)/shard_map/all_to_all | solution.py:201
  503.7 3.7 copy.87
  507.4 33.0 %all-gather.17.cloned.1.call-done = bf16[2048,512]{1,0:T(8,128)(2,1)} async-done(((bf16[256,512]{1,0:T(8,128)(2,1)}), bf16[2048,512]{1,0:T(8,128)(2,1)}) %all-gather.17.cloned.1.call-update) | async-done | bytes 2097168 | tf_op jit(solution)/shard_map/all_gather | solution.py:119
  540.5 6.2 %fusion.28 = bf16[768,512]{1,0:T(8,128)(2,1)} fusion(bf16[768,512]{1,0:T(8,128)(2,1)S(1)} %convolution_convert_fusion.2, bf16[768,2048]{1,0:T(8,128)(2,1)} %fusion.24, bf16[2048,512]{1,0:T(8,128)(2,1)} %all-gather.17.cloned.1.call-done, bf16[768,2,512]{2,0,1:T(8,128)(2,1)} %bitcast.190), kind=kOutput, calls=%fused_computation.47 | convolution fusion | flops 1616510976 | bytes 8388608 | tf_op jit(solution)/shard_map/dot_general | solution.py:123
  (320 shorter events, 159.1 us)
Async XLA Ops:
  6.5 86.9 %copy-start.6 = (f32[31,256]{1,0:T(8,128)S(1)}, f32[31,256]{1,0:T(8,128)}, u32[]{:S(2)}) copy-start(f32[31,256]{1,0:T(8,128)} %param.37) | copy-start | bytes 95236
  6.5 88.2 %copy-start.41 = (f32[256]{0:T(256)S(1)}, f32[256]{0:T(256)}, u32[]{:S(2)}) copy-start(f32[256]{0:T(256)} %param.33) | copy-start | bytes 3076
  6.5 45.0 %all-gather.31.cloned.1.call-start = ((), (), s32[]{:S(2)}) async-start(), calls=%async_computation.10 | async-start | bytes 1179648 | tf_op jit(solution)/shard_map/all_gather | solution.py:182
  7.3 84.8 %all-gather.35.cloned.1.call-start = ((), (), s32[]{:S(2)}) async-start(), calls=%async_computation.12 | async-start | bytes 1179648 | tf_op jit(solution)/shard_map/all_gather | solution.py:183
  8.0 113.1 %all-gather.15.cloned.1.call-start = ((), (), s32[]{:S(2)}) async-start(), calls=%async_computation.2 | async-start | bytes 3932160 | tf_op jit(solution)/shard_map/all_gather | solution.py:100
  8.7 154.7 %all-gather.19.cloned.1.call-start = ((), (), s32[]{:S(2)}) async-start(), calls=%async_computation.4 | async-start | bytes 1179648 | tf_op jit(solution)/shard_map/all_gather | solution.py:114
  9.3 195.1 %all-gather.23.cloned.1.call-start = ((), (), s32[]{:S(2)}) async-start(), calls=%async_computation.6 | async-start | bytes 1179648 | tf_op jit(solution)/shard_map/all_gather | solution.py:113
  9.9 235.5 %all-gather.21.cloned.1.call-start = ((), (), s32[]{:S(2)}) async-start(), calls=%async_computation.5 | async-start | bytes 1179648 | tf_op jit(solution)/shard_map/all_gather | solution.py:115
  10.5 113.4 %copy-start.7 = (f32[2048]{0:T(1024)S(1)}, f32[2048]{0:T(1024)}, u32[]{:S(2)}) copy-start(f32[2048]{0:T(1024)} %param.24) | copy-start | bytes 24580
  10.5 416.7 %all-gather.27.cloned.1.call-start = ((), (), s32[]{:S(2)}) async-start(), calls=%async_computation.8 | async-start | bytes 1179648 | tf_op jit(solution)/shard_map/all_gather | solution.py:117
  11.2 420.2 %all-gather.29.cloned.1.call-start = ((), (), s32[]{:S(2)}) async-start(), calls=%async_computation.9 | async-start | bytes 1179648 | tf_op jit(solution)/shard_map/all_gather | solution.py:118
  12.0 424.3 %all-gather.25.cloned.1.call-start = ((), (), s32[]{:S(2)}) async-start(), calls=%async_computation.7 | async-start | bytes 1179648 | tf_op jit(solution)/shard_map/all_gather | solution.py:116
  12.7 451.1 %all-gather.33.cloned.1.call-start = ((), (), s32[]{:S(2)}) async-start(), calls=%async_computation.11 | async-start | bytes 5242880 | tf_op jit(solution)/shard_map/all_gather | solution.py:187
  51.6 415.5 %all-gather.37.cloned.1.call-start = ((), (), s32[]{:S(2)}) async-start(), calls=%async_computation.13 | async-start | bytes 5242880 | tf_op jit(solution)/shard_map/all_gather | solution.py:188
  92.0 398.7 %all-gather.39.cloned.1.call-start = ((), (), s32[]{:S(2)}) async-start(), calls=%async_computation.14 | async-start | bytes 2359296 | tf_op jit(solution)/shard_map/all_gather | solution.py:120
  92.6 447.8 %all-gather.17.cloned.1.call-start = ((), (), s32[]{:S(2)}) async-start(), calls=%async_computation.3 | async-start | bytes 2359296 | tf_op jit(solution)/shard_map/all_gather | solution.py:119
  124.0 39.5 %copy-start.43 = (f32[768,256]{1,0:T(8,128)S(1)}, f32[768,256]{1,0:T(8,128)}, u32[]{:S(2)}) copy-start(f32[768,256]{1,0:T(8,128)} %param.34) | copy-start | bytes 2359300
  403.3 21.5 %copy-start.5 = (f32[2,128,128]{2,1,0:T(8,128)S(1)}, f32[2,128,128]{2,1,0:T(8,128)}, u32[]{:S(2)}) copy-start(f32[2,128,128]{2,1,0:T(8,128)} %param.35) | copy-start | bytes 393220
  403.4 22.4 %copy-start.42 = (f32[256]{0:T(256)S(1)}, f32[256]{0:T(256)}, u32[]{:S(2)}) copy-start(f32[256]{0:T(256)} %param.36) | copy-start | bytes 3076
  434.5 5.3 collective-permute-start
  440.2 9.0 %copy-start.39 = (f32[256]{0:T(256)S(1)}, f32[256]{0:T(256)}, u32[]{:S(2)}) copy-start(f32[256]{0:T(256)} %param.39) | copy-start | bytes 3076
  440.2 9.0 %copy-start.40 = (f32[256]{0:T(256)S(1)}, f32[256]{0:T(256)}, u32[]{:S(2)}) copy-start(f32[256]{0:T(256)} %param.38) | copy-start | bytes 3076
  440.2 9.3 %copy-start.4 = (bf16[768,256]{1,0:T(8,128)(2,1)S(1)}, bf16[768,256]{1,0:T(8,128)(2,1)}, u32[]{:S(2)}) copy-start(bf16[768,256]{1,0:T(8,128)(2,1)} %multiply_convert_fusion.1) | copy-start | bytes 1179652
  474.5 29.2 %all-to-all-start.1 = ((bf16[192,2,2048]{0,1,2:T(2,128)(2,1)}), bf16[192,2,2048]{0,1,2:T(2,128)(2,1)S(1)}, u32[]{:S(2)}, u32[]{:S(2)}) async-start(bf16[192,2,2048]{0,1,2:T(2,128)(2,1)} %copy.86), calls=%async_computation.1 | async-start | bytes 4194304 | tf_op jit(solution)/shard_map/all_to_all | solution.py:201
  (35 other events, 122.2 us)
Sparse Core Ops, SparseCore 0:
  9.4 42.1 all-gather.30
  53.6 38.3 all-gather.34
  93.6 27.5 all-gather.14
  123.1 40.2 all-gather.18
  165.4 38.9 all-gather.22
  206.4 38.9 all-gather.20
  247.6 38.9 all-gather.26
  288.7 38.9 all-gather.28
  329.9 38.9 all-gather.24
  370.3 33.1 all-gather.32
  405.1 34.4 all-gather.36
  441.6 49.0 all-gather.38
  492.8 47.5 all-gather.16
where the time goes:
time: 556 us; the launch traced here: 553 us
  waiting for transfers between devices  277 us (50%)
  matrix products  77.9 us (14%)
  blocking collectives  69.7 us (13%)
  other arithmetic  66.1 us (12%)
  local copies, waits for them, and re-layouts  41.3 us (7%)
  between operations  14.2 us (3%)
  starting transfers between devices  6.07 us (1%)
    all_gather x2, blocking collectives, prefix(): lax.all_gather(part.astype(kind), axis)  50 us
    dot_general x12, other arithmetic, block_step(): jnp.einsum('htd,hsd,htsd->hts', query, input_gate, weight, precision=high...  42.5 us
    all_gather x1, waiting for transfers between devices, local(): lax.all_gather(w_out_conv, 'sp', axis=1, tiled=True)  40.4 us
    all_gather x1, waiting for transfers between devices, local(): lax.all_gather(w_out_rec, 'sp', axis=1, tiled=True)  38.8 us
    all_gather x1, waiting for transfers between devices, local(): lax.all_gather(weights[1], 'sp', axis=0, tiled=True)  37 us
    all_gather x1, waiting for transfers between devices, local(): lax.all_gather(weights[0], 'sp', axis=0, tiled=True)  36.7 us
    all_gather x1, waiting for transfers between devices, local(): lax.all_gather(weights[2], 'sp', axis=0, tiled=True)  36.6 us
    all_gather x1, waiting for transfers between devices, local(): lax.all_gather(weights[6], 'sp', axis=0, tiled=True)  33 us
  transfers between devices with their start and end apart: 15, of which 9 were waited for; matrix products, arithmetic and copies ran while one was open for 32% of the time, Pallas kernels for 0%

commit v1 on v0

v1 whole, which is shorter than its diff:
```python
import functools

import jax
import jax.numpy as jnp
from jax import lax
from jax.experimental import pallas as pl
from jax.experimental.pallas import tpu as pltpu
from jax.sharding import PartitionSpec as P

HEAD = 128
CONV = 1024
KW = 31
BLOCK = 64
EPSILON = 1e-06
MESH = pl.DeviceIdType.MESH


def passed_along(block, axis, distance):
    devices = range(lax.axis_size(axis))
    route = [(i - distance, i) for i in devices if i - distance in devices]
    return lax.ppermute(block, axis, route)


def normalize_rows(values, gain_vector):
    widened = values.astype(jnp.float32)
    scale = lax.rsqrt(jnp.mean(widened * widened, axis=-1, keepdims=True) + EPSILON)
    return (widened * scale * gain_vector).astype(jnp.bfloat16)


def tp_partners(m):
    me = lax.axis_index("tp")
    core = me % 2
    chip = me // 2
    chips = m // 2
    others = [((chip + k) % chips) * 2 + core for k in range(1, chips)]
    sources = [((chip + chips - k) % chips) * 2 + core for k in range(1, chips)]
    sibling = chip * 2 + (1 - core)
    return me, others, sources, sibling


def remote(src, dst, send, recv, device):
    return pltpu.make_async_remote_copy(
        src_ref=src, dst_ref=dst, send_sem=send, recv_sem=recv, device_id=device, device_id_type=MESH
    )


def tp_start(own, out, m, send, recv, local_sem):
    me, others, sources, sibling = tp_partners(m)
    mine = pltpu.make_async_copy(own, out.at[me], local_sem)
    mine.start()
    started = []
    for k, other in enumerate(others):
        copy = remote(own, out.at[me], send.at[k], recv.at[k], {"tp": other})
        copy.start()
        started.append(copy)
    near = remote(own, out.at[me], send.at[m - 1], recv.at[m - 1], {"tp": sibling})
    near.start()
    return mine, started, near


def tp_forward(own, out, m, send, recv, state):
    mine, started, near = state
    me, others, sources, sibling = tp_partners(m)
    chips = m // 2
    handed = []
    for k, source in enumerate(sources):
        started[k].wait_recv()
        copy = remote(
            out.at[source],
            out.at[source],
            send.at[chips - 1 + k],
            recv.at[chips - 1 + k],
            {"tp": sibling},
        )
        copy.start()
        handed.append(copy)
    return mine, started, near, handed


def tp_finish(state):
    mine, started, near, handed = state
    for copy in started:
        copy.wait_send()
    near.wait()
    for copy in handed:
        copy.wait()
    mine.wait()


def greet(extra, m):
    me, others, sources, sibling = tp_partners(m)
    barrier = pltpu.get_barrier_semaphore()
    for other in others + [sibling]:
        pl.semaphore_signal(barrier, inc=1, device_id={"tp": other}, device_id_type=MESH)
    for device in extra:
        pl.semaphore_signal(barrier, inc=1, device_id={"sp": device}, device_id_type=MESH)
    pl.semaphore_wait(barrier, len(others) + 1 + len(extra))


def tp_gather_kernel(m, own, out, send, recv, local_sem):
    greet([], m)
    state = tp_start(own, out, m, send, recv, local_sem)
    tp_finish(tp_forward(own, out, m, send, recv, state))


def tp_gather(block, cid):
    m = lax.axis_size("tp")
    return pl.pallas_call(
        functools.partial(tp_gather_kernel, m),
        out_shape=jax.ShapeDtypeStruct((m,) + block.shape, block.dtype),
        in_specs=[pl.BlockSpec(memory_space=pl.ANY)],
        out_specs=pl.BlockSpec(memory_space=pl.ANY),
        scratch_shapes=[
            pltpu.SemaphoreType.DMA((m,)),
            pltpu.SemaphoreType.DMA((m,)),
            pltpu.SemaphoreType.DMA,
        ],
        compiler_params=pltpu.CompilerParams(collective_id=cid, has_side_effects=True),
    )(block)


def ring_kernel(n, m, w, tok, g, toks, wsend, wrecv, wlocal, tsend, trecv, tlocal):
    ny = n // 4 if n % 4 == 0 else 1
    nz = n // ny

    def place(index):
        z, y = index // ny, index % ny
        return y * nz + z + (y % 2) * (nz - 1 - 2 * z)

    def at(spot):
        spot = (spot + 2 * n) % n
        y, r = spot // nz, spot % nz
        return (r + (y % 2) * (nz - 1 - 2 * r)) * ny + y

    me = lax.axis_index("sp")
    pos = place(me)
    right, left = at(pos + 1), at(pos - 1)
    half = w.shape[0] // 2
    greet([right, left], m)
    mine = pltpu.make_async_copy(w, g.at[me], wlocal)
    mine.start()
    tstate = None
    copies = []
    for step in range(n - 1):
        for way, (device, sign) in enumerate(((right, -1), (left, 1))):
            rows = pl.ds(way * half, half)
            block = at(pos + sign * step)
            if step > 0:
                copies[2 * (step - 1) + way].wait_recv()
            copy = remote(
                w.at[rows] if step == 0 else g.at[block, rows],
                g.at[block, rows],
                wsend.at[step, way],
                wrecv.at[step, way],
                {"sp": device},
            )
            copy.start()
            copies.append(copy)
        if step == 0:
            tstate = tp_start(tok, toks, m, tsend, trecv, tlocal)
        if step == 2:
            tstate = tp_forward(tok, toks, m, tsend, trecv, tstate)
    for copy in copies[-2:]:
        copy.wait_recv()
    for copy in copies:
        copy.wait_send()
    mine.wait()
    tp_finish(tstate)


def ring_gather(w, tok):
    n, m = lax.axis_size("sp"), lax.axis_size("tp")
    return pl.pallas_call(
        functools.partial(ring_kernel, n, m),
        out_shape=(
            jax.ShapeDtypeStruct((n,) + w.shape, w.dtype),
            jax.ShapeDtypeStruct((m,) + tok.shape, tok.dtype),
        ),
        in_specs=[pl.BlockSpec(memory_space=pl.ANY)] * 2,
        out_specs=(pl.BlockSpec(memory_space=pl.ANY),) * 2,
        scratch_shapes=[
            pltpu.SemaphoreType.DMA((n - 1, 2)),
            pltpu.SemaphoreType.DMA((n - 1, 2)),
            pltpu.SemaphoreType.DMA,
            pltpu.SemaphoreType.DMA((m,)),
            pltpu.SemaphoreType.DMA((m,)),
            pltpu.SemaphoreType.DMA,
        ],
        compiler_params=pltpu.CompilerParams(collective_id=0, has_side_effects=True),
    )(w, tok)


def dot(a, b, dims):
    return lax.dot_general(a, b, (dims, ((), ())), preferred_element_type=jnp.float32)


def recurrence_kernel(q_ref, f_ref, i_ref, lb_ref, ds_ref, out_ref, qd_ref, st_ref, dec_ref):
    row = lax.broadcasted_iota(jnp.int32, (BLOCK, BLOCK), 0)
    col = lax.broadcasted_iota(jnp.int32, (BLOCK, BLOCK), 1)
    causal = row >= col
    lower = causal.astype(jnp.float32)
    slack = 1.0 - lb_ref[...]
    state = jnp.zeros((HEAD, HEAD), jnp.float32)
    run = jnp.zeros((1, HEAD), jnp.float32)
    for b in range(q_ref.shape[0] // BLOCK):
        rows = pl.ds(b * BLOCK, BLOCK)
        raw = q_ref[rows, :].astype(jnp.float32)
        query = raw * jax.nn.sigmoid(raw)
        gate = slack * jax.nn.sigmoid(-f_ref[rows, :].astype(jnp.float32))
        values = i_ref[rows, :]
        log_decay = jnp.log1p(-gate) + ds_ref[rows, :]
        cum = jnp.dot(
            lower, log_decay, precision=lax.Precision.HIGHEST, preferred_element_type=jnp.float32
        )
        final = cum[BLOCK - 1 :, :]
        qe = query * jnp.exp(cum)
        qb = qe.astype(jnp.bfloat16)
        ke = (gate * jnp.exp(-cum)).astype(jnp.bfloat16)
        scores = jnp.where(causal, dot(qb, ke, ((1,), (1,))), 0.0).astype(jnp.bfloat16)
        out = dot(scores, values, ((1,), (0,)))
        out_ref[rows, :] = out + dot(qb, state.astype(jnp.bfloat16), ((1,), (1,)))
        qd_ref[rows, :] = (qe * jnp.exp(run)).astype(jnp.bfloat16)
        kd = (gate * jnp.exp(final - cum)).astype(jnp.bfloat16)
        state = state * jnp.exp(final) + dot(values, kd, ((0,), (0,)))
        run = run + final
    st_ref[0] = state
    dec_ref[0] = jnp.exp(run)


def recurrence(raw, lower_bound, decay_shift, heads):
    rows = raw.shape[0]
    column = lambda k: pl.BlockSpec((rows, HEAD), lambda h: (0, k * heads + h))
    return pl.pallas_call(
        recurrence_kernel,
        grid=(heads,),
        out_shape=(
            jax.ShapeDtypeStruct((rows, heads * HEAD), jnp.float32),
            jax.ShapeDtypeStruct((rows, heads * HEAD), jnp.bfloat16),
            jax.ShapeDtypeStruct((heads, HEAD, HEAD), jnp.float32),
            jax.ShapeDtypeStruct((heads, 1, HEAD), jnp.float32),
        ),
        in_specs=[
            column(0),
            column(1),
            column(2),
            pl.BlockSpec((1, HEAD), lambda h: (0, h)),
            column(0),
        ],
        out_specs=(
            column(0),
            column(0),
            pl.BlockSpec((1, HEAD, HEAD), lambda h: (h, 0, 0)),
            pl.BlockSpec((1, 1, HEAD), lambda h: (h, 0, 0)),
        ),
    )(raw, raw, raw, lower_bound[None], decay_shift)


def local(
    tokens,
    norm_gain,
    w_query,
    w_forget,
    w_input,
    w_outgate,
    w_conv_value,
    w_conv_gate,
    w_gate_rec,
    w_gate_conv,
    lower_bound,
    decay_shift,
    state_init,
    head_gain,
    conv_kernel,
    channel_gain,
    channel_bias,
    w_out_rec,
    w_out_conv,
):
    n, m = lax.axis_size("sp"), lax.axis_size("tp")
    weights = (
        w_query,
        w_forget,
        w_input,
        w_outgate,
        w_conv_value,
        w_conv_gate,
        w_gate_rec,
        w_gate_conv,
        w_out_rec,
        w_out_conv,
    )
    width = w_query.shape[1]
    features = w_gate_rec.shape[1]
    gathered, rows_all = ring_gather(jnp.concatenate(weights, axis=1), tokens)
    inputs_width = 6 * width + 2 * features
    normed = normalize_rows(rows_all.reshape(-1, tokens.shape[1]), norm_gain)
    row_count = normed.shape[0]
    stacked = gathered.reshape(n * w_query.shape[0], -1)
    raw = jnp.dot(
        normed, stacked[:, :inputs_width], preferred_element_type=jnp.float32
    ).astype(jnp.bfloat16)
    out_w = gathered[:, :, inputs_width:].reshape(m, n // m, w_out_rec.shape[0], 2, -1)
    out_w = lax.all_to_all(out_w, "tp", split_axis=0, concat_axis=0, tiled=True)
    out_w = out_w.transpose(3, 0, 2, 1, 4).reshape(2, m * w_out_rec.shape[0], features)

    heads = width // HEAD
    local_out, decayed_query, local_state, forgetting = recurrence(
        raw, lower_bound, decay_shift, heads
    )
    states = lax.all_gather(local_state.astype(jnp.bfloat16), "sp").astype(jnp.float32)
    decays = lax.all_gather(forgetting.astype(jnp.bfloat16), "sp").astype(jnp.float32)
    position = lax.axis_index("sp")
    incoming = state_init.transpose(0, 2, 1)
    for k in range(n - 1):
        incoming = jnp.where(k < position, incoming * decays[k] + states[k], incoming)
    head_out = local_out.reshape(row_count, heads, HEAD) + jnp.einsum(
        "thd,hvd->thv",
        decayed_query.reshape(row_count, heads, HEAD),
        incoming.astype(jnp.bfloat16),
        preferred_element_type=jnp.float32,
    )
    head_out = head_out * lax.rsqrt(jnp.mean(head_out * head_out, axis=-1, keepdims=True) + EPSILON)
    head_out = head_out * head_gain.reshape(heads, HEAD)

    def part(k):
        return raw[:, k * width : (k + 1) * width].astype(jnp.float32)

    mixed_rec = (head_out.reshape(row_count, width) * jax.nn.silu(part(3))).astype(jnp.bfloat16)
    gated = (part(4) * jax.nn.sigmoid(part(5))).astype(jnp.bfloat16)
    rim_width = KW - 1
    previous = passed_along(gated[row_count - rim_width :], "sp", 1)
    extended = jnp.concatenate([previous, gated], axis=0).astype(jnp.float32)
    conv_out = jnp.zeros((row_count, width), jnp.float32)
    for tap_index in range(KW):
        conv_out = conv_out + conv_kernel[tap_index] * extended[tap_index : tap_index + row_count]
    squares = lax.psum(jnp.sum(conv_out * conv_out, axis=1), "tp")
    scale = lax.rsqrt(squares / CONV + EPSILON)[:, None]
    mixed_conv = jax.nn.silu(conv_out * scale * channel_gain + channel_bias).astype(jnp.bfloat16)

    both = tp_gather(jnp.concatenate([mixed_rec, mixed_conv], axis=1), 1)

    def project(branch):
        total = 0.0
        for t in range(m):
            total = total + jnp.dot(
                both[t, :, branch * width : (branch + 1) * width],
                out_w[branch, t * width : (t + 1) * width],
                preferred_element_type=jnp.float32,
            )
        return total.astype(jnp.bfloat16).astype(jnp.float32)

    gates = raw[:, 6 * width :].astype(jnp.float32)
    merged = jax.nn.sigmoid(gates[:, :features]) * project(0)
    merged = merged + jax.nn.sigmoid(gates[:, features:]) * project(1)
    return merged.astype(jnp.bfloat16)

def solution(mesh):
    in_specs = (
        P(("sp", "tp"), None),
        P(),
        P("sp", "tp"),
        P("sp", "tp"),
        P("sp", "tp"),
        P("sp", "tp"),
        P("sp", "tp"),
        P("sp", "tp"),
        P("sp", "tp"),
        P("sp", "tp"),
        P("tp"),
        P("sp", "tp"),
        P("tp", None, None),
        P("tp"),
        P(None, "tp"),
        P("tp"),
        P("tp"),
        P("tp", "sp"),
        P("tp", "sp"),
    )
    out_specs = P("sp", "tp")
    return jax.shard_map(local, mesh=mesh, in_specs=in_specs, out_specs=out_specs, check_vma=False)
```

time: 556 us -> 298 us (0.54)
  waiting for transfers between devices: 277 us -> 0.01 us
  Pallas kernels: 0 us -> 163 us
  matrix products: 77.9 us -> 18.1 us
  other arithmetic: 66.1 us -> 13.6 us
  local copies, waits for them, and re-layouts: 41.3 us -> 27.2 us
  between operations: 14.2 us -> 0.42 us
    all_gather x13 -> x0, waiting for transfers between devices: 261 us -> none  [the longest x1 40.4 us: local(): lax.all_gather(w_out_conv, 'sp', axis=1, tiled=True)]
    pallas_call x0 -> x3, Pallas kernels: none -> 163 us  [the longest x1 127 us: ring_gather(): pl.pallas_call(functools.partial(ring_kernel, n, m), out_shape=(jax.Shape...]
    dot_general x47 -> x10, matrix products: 77.9 us -> 18.1 us  [the longest x1 12.3 us: local(): jnp.dot(normed, stacked[:, :inputs_width], preferred_element_type=jnp.flo...]
    dot_general x12 -> x0, other arithmetic: 42.5 us -> none  [block_step(): jnp.einsum('htd,hsd,htsd->hts', query, input_gate, weight, precision=high...]
    squeeze x24 -> x0, local copies, waits for them, and re-layouts: 20.9 us -> none  [local(): lax.scan(block_step, zero_state, (to_blocks(query), to_blocks(input_gate)...]
    psum x1, blocking collectives: 5.67 us -> 20 us  [local(): squares = lax.psum(jnp.sum(conv_out * conv_out, axis=1), 'tp')]
    all_to_all x1 -> x0, blocking collectives: 14.1 us -> none  [local(): lax.all_to_all(both, 'tp', split_axis=0, concat_axis=2, tiled=True)]
    select_n x28 -> x0, other arithmetic: 12.2 us -> none  [the longest x12 11 us: block_step(): jnp.where(causal_masked, jnp.exp(jnp.where(causal_masked, spread, 0.0)),...]
  transfers between devices with their start and end apart: 15 -> 2, of which waited for: 9 -> 0; matrix products, arithmetic and copies ran while one was open for 32% -> 6% of each run, Pallas kernels for 0% -> 9%
where the time goes in v1:
time: 298 us
  Pallas kernels  163 us (55%)
  blocking collectives  70.1 us (24%)
  local copies, waits for them, and re-layouts  27.2 us (9%)
  matrix products  18.1 us (6%)
  other arithmetic  13.6 us (5%)
  starting transfers between devices  5.08 us (2%)
    pallas_call x1, Pallas kernels, ring_gather(): pl.pallas_call(functools.partial(ring_kernel, n, m), out_shape=(jax.Shape...  127 us
    all_gather x1, blocking collectives, local(): lax.all_gather(local_state.astype(jnp.bfloat16), 'sp').astype(jnp.float32)  31.3 us
    pallas_call x1, Pallas kernels, tp_gather(): pl.pallas_call(functools.partial(tp_gather_kernel, m), out_shape=jax.Shap...  26.6 us
    psum x1, blocking collectives, local(): squares = lax.psum(jnp.sum(conv_out * conv_out, axis=1), 'tp')  20 us
    all_gather x1, blocking collectives, local(): lax.all_gather(forgetting.astype(jnp.bfloat16), 'sp').astype(jnp.float32)  18.8 us
    dot_general x1, matrix products, local(): jnp.dot(normed, stacked[:, :inputs_width], preferred_element_type=jnp.flo...  12.3 us
    pallas_call x1, Pallas kernels, recurrence(): pl.pallas_call(recurrence_kernel, grid=(heads,), out_shape=(jax.ShapeDtyp...  9.67 us
    unnamed x46, local copies, waits for them, and re-layouts  8.78 us
  transfers between devices with their start and end apart: 2, of which 0 were waited for; matrix products, arithmetic and copies ran while one was open for 6% of the time, Pallas kernels for 9%

profile of v1, /device:TPU:0, one launch (start us, length us, event | category | flops | bytes accessed | tf_op | source)
XLA Modules:
  0.0 297.8 jit_solution(4309060119103653480)
XLA Ops:
  0.0 1.1 copy.29
  5.9 1.1 copy-done.4
  7.0 127.0 %shard_map.181 = (bf16[8,256,3072]{2,1,0:T(8,128)(2,1)}, bf16[4,192,2048]{2,1,0:T(8,128)(2,1)}) custom-call(bf16[256,3072]{1,0:T(8,128)(2,1)} %copy-done.4, bf16[192,2048]{1,0:T(8,128)(2,1)} %tok.1), custom_call_target="tpu_custom_call" | custom-call | tf_op jit(solution)/shard_map/pallas_call | solution.py:173
  134.0 2.7 multiply_reduce_fusion
  137.7 12.3 %fusion.4.q_ref.f_ref.i_ref = bf16[768,2560]{1,0:T(8,128)(2,1)} fusion(bf16[768,2048]{1,0:T(8,128)(2,1)S(1)} %fusion.3, bf16[2048,3072]{1,0:T(8,128)(2,1)} %bitcast.125), kind=kOutput, calls=%fused_computation.6 | convolution fusion | flops 8055029760 | bytes 17563648 | tf_op jit(solution)/shard_map/dot_general | solution.py:299
  149.9 9.7 %shard_map.182 = (f32[768,256]{1,0:T(8,128)}, bf16[768,256]{1,0:T(8,128)(2,1)}, f32[2,128,128]{2,1,0:T(8,128)}, f32[2,1,128]{2,1,0:T(1,128)}) custom-call(bf16[768,2560]{1,0:T(8,128)(2,1)} %fusion.4.q_ref.f_ref.i_ref, bf16[768,2560]{1,0:T(8,128)(2,1)} %fusion.4.q_ref.f_ref.i_ref, bf16[768,2560]{1,0:T(8,128)(2,1)} %fusion.4.q_ref.f_ref.i_ref, ...), custom_call_target="tpu_custom_call" | custom-call | tf_op jit(solution)/shard_map/pallas_call | solution.py:233
  159.6 1.4 copy.35
  161.1 18.8 %all-gather = bf16[16,1,128]{2,1,0:T(2,128)(2,1)S(1)} all-gather(bf16[2,1,128]{2,1,0:T(2,128)(2,1)S(1)} %convert_element_type.75), channel_id=2, replica_groups=mesh['sp'=8,'tp'=4] {'sp'}, dimensions={0}, use_global_device_ids=true | all-gather | bytes 4608 | tf_op jit(solution)/shard_map/all_gather | solution.py:311
  179.9 31.3 %all-gather.1 = bf16[16,128,128]{2,1,0:T(8,128)(2,1)S(1)} all-gather(bf16[2,128,128]{2,1,0:T(8,128)(2,1)S(1)} %convert_element_type.77), channel_id=3, replica_groups=mesh['sp'=8,'tp'=4] {'sp'}, dimensions={0}, use_global_device_ids=true | all-gather | bytes 589824 | tf_op jit(solution)/shard_map/all_gather | solution.py:310
  212.3 1.7 fusion.52
  214.0 1.3 collective-permute-start
  215.3 1.8 slice.387
  217.1 2.1 reshape.62
  219.3 5.1 %copy.33 = bf16[4,2,256,2,256]{4,1,2,3,0:T(2,128)(2,1)} copy(bf16[4,2,256,2,256]{4,3,2,1,0:T(2,128)(2,1)} %reshape.62) | data formatting | bytes 4194304 | tf_op jit(solution)/shard_map/reshape | solution.py:302
  224.4 3.8 %all-to-all-start = ((bf16[4,2,256,2,256]{4,1,2,3,0:T(2,128)(2,1)}), bf16[4,2,256,2,256]{4,1,2,3,0:T(2,128)(2,1)S(1)}, u32[]{:S(2)}, u32[]{:S(2)}) async-start(bf16[4,2,256,2,256]{4,1,2,3,0:T(2,128)(2,1)} %copy.33), calls=%async_computation | async-start | bytes 4194304 | tf_op jit(solution)/shard_map/all_to_all | solution.py:303
  228.2 3.5 %slice_convert_fusion = f32[768,1024]{1,0:T(8,128)} fusion(bf16[768,2560]{1,0:T(8,128)(2,1)} %fusion.4.q_ref.f_ref.i_ref), kind=kLoop, calls=%fused_computation.18 | loop fusion | flops 786432 | bytes 4718592 | tf_op jit(solution)/shard_map/convert_element_type | solution.py:352
  231.8 3.3 %multiply_reduce_fusion.1 = (f32[768]{0:T(1024)S(1)}, f32[768,256]{1,0:T(8,128)S(1)}) fusion(f32[798,256]{1,0:T(8,128)S(1)} %maximum_convert_fusion, f32[256]{0:T(256)S(1)} %bitcast.162, f32[256]{0:T(256)S(1)} %bitcast.163, f32[256]{0:T(256)S(1)} %bitcast.134, f32[256]{0:T(256)S(1)} %bitcast.135, f32[256]{0:T(256)S(1)} %bitcast.136, f32[256]{0:T(256)S(1)} %bitcast.137, ...), kind=kLoop, calls=%fused_computation.93 | loop fusion | flops 12385536 | bytes 25200640 | tf_op jit(solution)/shard_map/reduce_sum | solution.py:336
  235.1 20.0 %psum.7 = f32[768]{0:T(1024)S(1)} all-reduce(f32[768]{0:T(1024)S(1)} %get-tuple-element.17), channel_id=1, replica_groups=mesh['sp'=8,'tp'=4] {'tp'}, use_global_device_ids=true, to_apply=%region_3.4 | all-reduce | flops 768 | bytes 6144 | tf_op jit(solution)/shard_map/psum | solution.py:336
  256.4 26.6 %shard_map.183 = bf16[4,768,512]{2,1,0:T(8,128)(2,1)} custom-call(bf16[768,512]{1,0:T(8,128)(2,1)} %pad_maximum_fusion.own), custom_call_target="tpu_custom_call" | custom-call | tf_op jit(solution)/shard_map/pallas_call | solution.py:108
  283.0 3.0 %copy.34 = bf16[2,4,256,2,256]{4,3,2,1,0:T(2,128)(2,1)} copy(bf16[2,4,256,2,256]{4,3,2,0,1:T(2,128)(2,1)S(1)} %bitcast.122) | data formatting | bytes 4194304 | tf_op jit(solution)/shard_map/transpose | solution.py:304
  286.0 4.6 %reshape.63 = bf16[2,1024,512]{2,1,0:T(8,128)(2,1)} reshape(bf16[2,4,256,2,256]{4,3,2,1,0:T(2,128)(2,1)} %copy.34) | data formatting | bytes 4194304 | tf_op jit(solution)/shard_map/reshape | solution.py:304
  290.6 1.5 fusion.56
  294.6 1.4 copy-done.3
  296.0 1.8 fusion.16
  (70 shorter events, 10.5 us)
Async XLA Ops:
  0.0 5.7 %copy-start.9 = (bf16[256,256]{1,0:T(8,128)(2,1)S(1)}, bf16[256,256]{1,0:T(8,128)(2,1)}, u32[]{:S(2)}) copy-start(bf16[256,256]{1,0:T(8,128)(2,1)} %param.26) | copy-start | bytes 393220
  0.0 5.7 %copy-start.6 = (bf16[256,512]{1,0:T(8,128)(2,1)S(1)}, bf16[256,512]{1,0:T(8,128)(2,1)}, u32[]{:S(2)}) copy-start(bf16[256,512]{1,0:T(8,128)(2,1)} %param.27) | copy-start | bytes 786436
  0.0 5.8 %copy-start.7 = (bf16[256,512]{1,0:T(8,128)(2,1)S(1)}, bf16[256,512]{1,0:T(8,128)(2,1)}, u32[]{:S(2)}) copy-start(bf16[256,512]{1,0:T(8,128)(2,1)} %param.28) | copy-start | bytes 786436
  0.0 5.8 %copy-start.10 = (bf16[256,256]{1,0:T(8,128)(2,1)S(1)}, bf16[256,256]{1,0:T(8,128)(2,1)}, u32[]{:S(2)}) copy-start(bf16[256,256]{1,0:T(8,128)(2,1)} %param.36) | copy-start | bytes 393220
  0.0 5.8 %copy-start.11 = (bf16[256,256]{1,0:T(8,128)(2,1)S(1)}, bf16[256,256]{1,0:T(8,128)(2,1)}, u32[]{:S(2)}) copy-start(bf16[256,256]{1,0:T(8,128)(2,1)} %param.37) | copy-start | bytes 393220
  5.9 1.1 copy-start.4
  134.0 2.8 copy-start
  134.0 2.8 copy-start.13
  159.6 1.5 copy-start.16
  159.6 20.3 %copy-start.8 = (f32[2,128,128]{2,1,0:T(8,128)S(1)}, f32[2,128,128]{2,1,0:T(8,128)}, u32[]{:S(2)}) copy-start(f32[2,128,128]{2,1,0:T(8,128)} %get-tuple-element.15) | copy-start | bytes 393220
  161.1 50.2 %copy-start.5 = (bf16[768,256]{1,0:T(8,128)(2,1)S(1)}, bf16[768,256]{1,0:T(8,128)(2,1)}, u32[]{:S(2)}) copy-start(bf16[768,256]{1,0:T(8,128)(2,1)} %get-tuple-element.16) | copy-start | bytes 1179652
  211.2 0.7 copy-start.17
  214.0 17.7 %collective-permute-start = (bf16[30,256]{1,0:T(8,128)(2,1)S(1)}, bf16[30,256]{1,0:T(8,128)(2,1)S(1)}, u32[]{:S(2)}, u32[]{:S(2)}) collective-permute-start(bf16[30,256]{1,0:T(8,128)(2,1)S(1)} %slice.438), channel_id=1, source_target_pairs={{0,4},{4,8},{8,12},{12,16},{16,20},{20,24},{24,28},{1,5},{5,9},{9,... | collective-permute-start | bytes 46088 | tf_op jit(solution)/shard_map/ppermute | solution.py:21
  224.4 58.6 %all-to-all-start = ((bf16[4,2,256,2,256]{4,1,2,3,0:T(2,128)(2,1)}), bf16[4,2,256,2,256]{4,1,2,3,0:T(2,128)(2,1)S(1)}, u32[]{:S(2)}, u32[]{:S(2)}) async-start(bf16[4,2,256,2,256]{4,1,2,3,0:T(2,128)(2,1)} %copy.33), calls=%async_computation | async-start | bytes 4194304 | tf_op jit(solution)/shard_map/all_to_all | solution.py:303
  228.2 3.5 %copy-start.12 = (f32[31,256]{1,0:T(8,128)S(1)}, f32[31,256]{1,0:T(8,128)}, u32[]{:S(2)}) copy-start(f32[31,256]{1,0:T(8,128)} %param.33) | copy-start | bytes 95236
  231.8 23.3 %copy-start.14 = (f32[256]{0:T(256)S(1)}, f32[256]{0:T(256)}, u32[]{:S(2)}) copy-start(f32[256]{0:T(256)} %param.35) | copy-start | bytes 3076
  231.8 23.3 %copy-start.15 = (f32[256]{0:T(256)S(1)}, f32[256]{0:T(256)}, u32[]{:S(2)}) copy-start(f32[256]{0:T(256)} %param.34) | copy-start | bytes 3076
  286.0 4.6 %copy-start.1 = (bf16[4,768,512]{2,1,0:T(8,128)(2,1)S(1)}, bf16[4,768,512]{2,1,0:T(8,128)(2,1)}, u32[]{:S(2)}) copy-start(bf16[4,768,512]{2,1,0:T(8,128)(2,1)} %shard_map.183) | copy-start | bytes 9437188
  290.6 1.7 copy-start.2
  294.1 1.9 copy-start.3

commit v2 on v1

--- a/solution.py
+++ b/solution.py
@@ -13,12 +13,6 @@
 BLOCK = 64
 EPSILON = 1e-06
 MESH = pl.DeviceIdType.MESH
-
-
-def passed_along(block, axis, distance):
-    devices = range(lax.axis_size(axis))
-    route = [(i - distance, i) for i in devices if i - distance in devices]
-    return lax.ppermute(block, axis, route)
 
 
 def normalize_rows(values, gain_vector):
@@ -119,7 +113,9 @@
     )(block)
 
 
-def ring_kernel(n, m, w, tok, g, toks, wsend, wrecv, wlocal, tsend, trecv, tlocal):
+def ring_kernel(
+    n, m, first, w, tok, g, toks, ow, wsend, wrecv, wlocal, tsend, trecv, tlocal, osend, orecv
+):
     ny = n // 4 if n % 4 == 0 else 1
     nz = n // ny
 
@@ -136,7 +132,27 @@
     pos = place(me)
     right, left = at(pos + 1), at(pos - 1)
     half = w.shape[0] // 2
-    greet([right, left], m)
+    tp = lax.axis_index("tp")
+    share = n // m
+    columns = pl.ds(first, w.shape[1] - first)
+    handed = []
+
+    def hand(block, way):
+        owner, slot, rows = block // share, block % share, pl.ds(way * half, half)
+        copy = remote(
+            g.at[block, rows, columns],
+            ow.at[tp, slot, rows],
+            osend.at[len(handed)],
+            orecv.at[tp, slot, way],
+            {"tp": owner},
+        )
+        handed.append((owner, copy))
+
+        @pl.when(owner != tp)
+        def _():
+            copy.start()
+
+    greet_all([right, left], m)
     mine = pltpu.make_async_copy(w, g.at[me], wlocal)
     mine.start()
     tstate = None
@@ -156,35 +172,113 @@
             )
             copy.start()
             copies.append(copy)
+            if step > 0:
+                hand(block, way)
         if step == 0:
             tstate = tp_start(tok, toks, m, tsend, trecv, tlocal)
         if step == 2:
             tstate = tp_forward(tok, toks, m, tsend, trecv, tstate)
-    for copy in copies[-2:]:
-        copy.wait_recv()
+            mine.wait()
+            for way in range(2):
+                hand(me, way)
+    for way, sign in enumerate((-1, 1)):
+        copies[2 * (n - 2) + way].wait_recv()
+        hand(at(pos + sign * (n - 1)), way)
     for copy in copies:
         copy.wait_send()
+    tp_finish(tstate)
+    for owner, copy in handed:
+
+        @pl.when(owner != tp)
+        def _(copy=copy):
+            copy.wait_send()
+
+    for k in range(1, m):
+        source = (tp + k) % m
+        for slot in range(share):
+            for way in range(2):
+                rows = pl.ds(way * half, half)
+                landed = ow.at[source, slot, rows]
+                remote(
+                    landed, landed, osend.at[0], orecv.at[source, slot, way], {"tp": source}
+                ).wait_recv()
+
+
+def greet_all(extra, m):
+    me = lax.axis_index("tp")
+    barrier = pltpu.get_barrier_semaphore()
+    for k in range(1, m):
+        pl.semaphore_signal(
+            barrier, inc=1, device_id={"tp": (me + k) % m}, device_id_type=MESH
+        )
+    for device in extra:
+        pl.semaphore_signal(barrier, inc=1, device_id={"sp": device}, device_id_type=MESH)
+    pl.semaphore_wait(barrier, m - 1 + len(extra))
+
+
+def exchange_kernel(n, own, rim, out, before, send, recv, rsend, rrecv, local_sem):
+    me = lax.axis_index("sp")
+    barrier = pltpu.get_barrier_semaphore()
+    for k in range(1, n):
+        pl.semaphore_signal(
+            barrier, inc=1, device_id={"sp": (me + k) % n}, device_id_type=MESH
+        )
+    mine = pltpu.make_async_copy(own, out.at[me], local_sem)
+    mine.start()
+    pl.semaphore_wait(barrier, n - 1)
+    copies = [remote(rim, before, rsend, rrecv, {"sp": (me + 1) % n})]
+    for k in range(1, n):
+        copies.append(
+            remote(own, out.at[me], send.at[k - 1], recv.at[k - 1], {"sp": (me + k) % n})
+        )
+    for copy in copies:
+        copy.start()
+    for copy in copies:
+        copy.wait()
     mine.wait()
-    tp_finish(tstate)
-
-
-def ring_gather(w, tok):
-    n, m = lax.axis_size("sp"), lax.axis_size("tp")
+
+
+def exchange(own, rim):
+    n = lax.axis_size("sp")
     return pl.pallas_call(
-        functools.partial(ring_kernel, n, m),
+        functools.partial(exchange_kernel, n),
         out_shape=(
-            jax.ShapeDtypeStruct((n,) + w.shape, w.dtype),
-            jax.ShapeDtypeStruct((m,) + tok.shape, tok.dtype),
+            jax.ShapeDtypeStruct((n,) + own.shape, own.dtype),
+            jax.ShapeDtypeStruct(rim.shape, rim.dtype),
         ),
         in_specs=[pl.BlockSpec(memory_space=pl.ANY)] * 2,
         out_specs=(pl.BlockSpec(memory_space=pl.ANY),) * 2,
         scratch_shapes=[
+            pltpu.SemaphoreType.DMA((n - 1,)),
+            pltpu.SemaphoreType.DMA((n - 1,)),
+            pltpu.SemaphoreType.DMA,
+            pltpu.SemaphoreType.DMA,
+            pltpu.SemaphoreType.DMA,
+        ],
+        compiler_params=pltpu.CompilerParams(collective_id=3, has_side_effects=True),
+    )(own, rim)
+
+
+def ring_gather(w, tok, first):
+    n, m = lax.axis_size("sp"), lax.axis_size("tp")
+    return pl.pallas_call(
+        functools.partial(ring_kernel, n, m, first),
+        out_shape=(
+            jax.ShapeDtypeStruct((n,) + w.shape, w.dtype),
+            jax.ShapeDtypeStruct((m,) + tok.shape, tok.dtype),
+            jax.ShapeDtypeStruct((m, n // m, w.shape[0], w.shape[1] - first), w.dtype),
+        ),
+        in_specs=[pl.BlockSpec(memory_space=pl.ANY)] * 2,
+        out_specs=(pl.BlockSpec(memory_space=pl.ANY),) * 3,
+        scratch_shapes=[
             pltpu.SemaphoreType.DMA((n - 1, 2)),
             pltpu.SemaphoreType.DMA((n - 1, 2)),
             pltpu.SemaphoreType.DMA,
             pltpu.SemaphoreType.DMA((m,)),
             pltpu.SemaphoreType.DMA((m,)),
             pltpu.SemaphoreType.DMA,
+            pltpu.SemaphoreType.DMA((2 * n,)),
+            pltpu.SemaphoreType.DMA((m, n // m, 2)),
         ],
         compiler_params=pltpu.CompilerParams(collective_id=0, has_side_effects=True),
     )(w, tok)
@@ -291,25 +385,40 @@
     )
     width = w_query.shape[1]
     features = w_gate_rec.shape[1]
-    gathered, rows_all = ring_gather(jnp.concatenate(weights, axis=1), tokens)
     inputs_width = 6 * width + 2 * features
+    gathered, rows_all, out_w = ring_gather(
+        jnp.concatenate(weights, axis=1), tokens, inputs_width
+    )
     normed = normalize_rows(rows_all.reshape(-1, tokens.shape[1]), norm_gain)
     row_count = normed.shape[0]
     stacked = gathered.reshape(n * w_query.shape[0], -1)
     raw = jnp.dot(
         normed, stacked[:, :inputs_width], preferred_element_type=jnp.float32
     ).astype(jnp.bfloat16)
-    out_w = gathered[:, :, inputs_width:].reshape(m, n // m, w_out_rec.shape[0], 2, -1)
-    out_w = lax.all_to_all(out_w, "tp", split_axis=0, concat_axis=0, tiled=True)
-    out_w = out_w.transpose(3, 0, 2, 1, 4).reshape(2, m * w_out_rec.shape[0], features)
+    share = n // m
+    me = lax.axis_index("tp")
+    own_w = lax.dynamic_slice_in_dim(gathered, me * share, share, 0)[:, :, inputs_width:]
+    out_w = lax.dynamic_update_slice_in_dim(out_w, own_w[None], me, 0)
+    out_rows, out_columns = w_out_rec.shape
+
+    def part(k):
+        return raw[:, k * width : (k + 1) * width].astype(jnp.float32)
+
+    gated = (part(4) * jax.nn.sigmoid(part(5))).astype(jnp.bfloat16)
 
     heads = width // HEAD
     local_out, decayed_query, local_state, forgetting = recurrence(
         raw, lower_bound, decay_shift, heads
     )
-    states = lax.all_gather(local_state.astype(jnp.bfloat16), "sp").astype(jnp.float32)
-    decays = lax.all_gather(forgetting.astype(jnp.bfloat16), "sp").astype(jnp.float32)
+    handover = jnp.concatenate(
+        [local_state, jnp.broadcast_to(forgetting, (heads, 16, HEAD))], axis=1
+    ).astype(jnp.bfloat16)
+    rim_width = KW - 1
+    everything, previous = exchange(handover, gated[row_count - 32 :])
+    everything = everything.astype(jnp.float32)
+    states, decays = everything[:, :, :HEAD], everything[:, :, HEAD : HEAD + 1]
     position = lax.axis_index("sp")
+    previous = jnp.where(position > 0, previous[32 - rim_width :], 0)
     incoming = state_init.transpose(0, 2, 1)
     for k in range(n - 1):
         incoming = jnp.where(k < position, incoming * decays[k] + states[k], incoming)
@@ -322,32 +431,31 @@
     head_out = head_out * lax.rsqrt(jnp.mean(head_out * head_out, axis=-1, keepdims=True) + EPSILON)
     head_out = head_out * head_gain.reshape(heads, HEAD)
 
-    def part(k):
-        return raw[:, k * width : (k + 1) * width].astype(jnp.float32)
-
     mixed_rec = (head_out.reshape(row_count, width) * jax.nn.silu(part(3))).astype(jnp.bfloat16)
-    gated = (part(4) * jax.nn.sigmoid(part(5))).astype(jnp.bfloat16)
-    rim_width = KW - 1
-    previous = passed_along(gated[row_count - rim_width :], "sp", 1)
     extended = jnp.concatenate([previous, gated], axis=0).astype(jnp.float32)
     conv_out = jnp.zeros((row_count, width), jnp.float32)
     for tap_index in range(KW):
         conv_out = conv_out + conv_kernel[tap_index] * extended[tap_index : tap_index + row_count]
-    squares = lax.psum(jnp.sum(conv_out * conv_out, axis=1), "tp")
+    squares = tp_gather(jnp.sum(conv_out * conv_out, axis=1).reshape(-1, HEAD), 2)
+    squares = jnp.sum(squares, axis=0).reshape(row_count)
     scale = lax.rsqrt(squares / CONV + EPSILON)[:, None]
     mixed_conv = jax.nn.silu(conv_out * scale * channel_gain + channel_bias).astype(jnp.bfloat16)
 
     both = tp_gather(jnp.concatenate([mixed_rec, mixed_conv], axis=1), 1)
 
     def project(branch):
-        total = 0.0
-        for t in range(m):
-            total = total + jnp.dot(
-                both[t, :, branch * width : (branch + 1) * width],
-                out_w[branch, t * width : (t + 1) * width],
-                preferred_element_type=jnp.float32,
-            )
-        return total.astype(jnp.bfloat16).astype(jnp.float32)
+        first = branch * out_columns
+        blocks = []
+        for j in range(share):
+            total = 0.0
+            for t in range(m):
+                total = total + jnp.dot(
+                    both[t, :, branch * width : (branch + 1) * width],
+                    out_w[t, j, :, first : first + out_columns],
+                    preferred_element_type=jnp.float32,
+                )
+            blocks.append(total.astype(jnp.bfloat16))
+        return jnp.concatenate(blocks, axis=1).astype(jnp.float32)
 
     gates = raw[:, 6 * width :].astype(jnp.float32)
     merged = jax.nn.sigmoid(gates[:, :features]) * project(0)

time: 298 us -> 244 us (0.82)
  blocking collectives: 70.1 us -> 0 us
  Pallas kernels: 163 us -> 188 us
  local copies, waits for them, and re-layouts: 27.2 us -> 17.2 us
  starting transfers between devices: 5.08 us -> 0 us
  other arithmetic: 13.6 us -> 17.5 us
    all_gather x2 -> x0, blocking collectives: 50.1 us -> none  [the longest x1 31.3 us: local(): lax.all_gather(local_state.astype(jnp.bfloat16), 'sp').astype(jnp.float32)]
    pallas_call x1 -> x2, Pallas kernels: 127 us -> 148 us  [the longest x1 135 us: ring_gather(): pl.pallas_call(functools.partial(ring_kernel, n, m, first), out_shape=(ja...]
    psum x1 -> x0, blocking collectives: 20 us -> none  [local(): squares = lax.psum(jnp.sum(conv_out * conv_out, axis=1), 'tp')]
    reshape x3 -> x0, local copies, waits for them, and re-layouts: 11.8 us -> none  [the longest x2 7.24 us: local(): gathered[:, :, inputs_width:].reshape(m, n // m, w_out_rec.shape[0], 2, -1)]
    pallas_call x1 -> x2, Pallas kernels: 26.6 us -> 30.5 us  [tp_gather(): pl.pallas_call(functools.partial(tp_gather_kernel, m), out_shape=jax.Shap...]
    all_to_all x1 -> x0, starting transfers between devices: 3.79 us -> none  [local(): out_w = lax.all_to_all(out_w, 'tp', split_axis=0, concat_axis=0, tiled=True)]
    transpose x1 -> x0, local copies, waits for them, and re-layouts: 3 us -> none  [local(): out_w.transpose(3, 0, 2, 1, 4).reshape(2, m * w_out_rec.shape[0], features)]
    dot_general x8 -> x16, matrix products: 5.56 us -> 7.4 us  [project(): jnp.dot(both[t, :, branch * width:(branch + 1) * width], out_w[t, j, :, f...]
  transfers between devices with their start and end apart: 2 -> 0, of which waited for: 0 -> 0; matrix products, arithmetic and copies ran while one was open for 6% -> 0% of each run, Pallas kernels for 9% -> 0%
where the time goes in v2:
time: 244 us; the launch traced here: 242 us
  Pallas kernels  188 us (77%)
  matrix products  18.8 us (8%)
  other arithmetic  17.5 us (7%)
  local copies, waits for them, and re-layouts  17.2 us (7%)
    pallas_call x1, Pallas kernels, ring_gather(): pl.pallas_call(functools.partial(ring_kernel, n, m, first), out_shape=(ja...  135 us
    pallas_call x2, Pallas kernels, tp_gather(): pl.pallas_call(functools.partial(tp_gather_kernel, m), out_shape=jax.Shap...  30.5 us
    pallas_call x1, Pallas kernels, exchange(): pl.pallas_call(functools.partial(exchange_kernel, n), out_shape=(jax.Shap...  13 us
    dot_general x1, matrix products, local(): jnp.dot(normed, stacked[:, :inputs_width], preferred_element_type=jnp.flo...  11.1 us
    unnamed x41, local copies, waits for them, and re-layouts  9.87 us
    pallas_call x1, Pallas kernels, recurrence(): pl.pallas_call(recurrence_kernel, grid=(heads,), out_shape=(jax.ShapeDtyp...  9.65 us
    dot_general x16, matrix products, project(): jnp.dot(both[t, :, branch * width:(branch + 1) * width], out_w[t, j, :, f...  7.4 us

profile of v2, /device:TPU:0, one launch (start us, length us, event | category | flops | bytes accessed | tf_op | source)
XLA Modules:
  0.0 241.8 jit_solution(4575457289816048088)
XLA Ops:
  0.0 1.1 fusion.129
  1.1 1.0 fusion.128
  2.1 1.0 copy.40
  4.1 0.9 constant_dynamic-update-slice_fusion.8
  5.9 0.9 constant_dynamic-update-slice_fusion.6
  8.8 1.2 copy-done.4
  10.0 134.6 %shard_map.181 = (bf16[8,256,3072]{2,1,0:T(8,128)(2,1)}, bf16[4,192,2048]{2,1,0:T(8,128)(2,1)}, bf16[4,2,256,512]{3,2,1,0:T(8,128)(2,1)}) custom-call(bf16[256,3072]{1,0:T(8,128)(2,1)} %copy-done.4, bf16[192,2048]{1,0:T(8,128)(2,1)} %tok.1), custom_call_target="tpu_custom_call" | custom-call | tf_op jit(solution)/shard_map/pallas_call | solution.py:264
  144.7 2.1 fusion.57
  146.7 2.6 %multiply_reduce_fusion = f32[4,192]{1,0:T(4,128)S(1)} fusion(bf16[4,192,2048]{2,1,0:T(8,128)(2,1)} %get-tuple-element.14), kind=kLoop, calls=%fused_computation.5 | loop fusion | flops 4717824 | bytes 3148800 | tf_op jit(solution)/shard_map/reduce_sum | solution.py:20
  150.2 11.1 %fusion.4.q_ref.f_ref.i_ref = bf16[768,2560]{1,0:T(8,128)(2,1)S(1)} fusion(bf16[768,2048]{1,0:T(8,128)(2,1)S(1)} %fusion.3, bf16[2048,3072]{1,0:T(8,128)(2,1)} %bitcast.250), kind=kOutput, calls=%fused_computation.6 | convolution fusion | flops 8055029760 | bytes 17563648 | tf_op jit(solution)/shard_map/dot_general | solution.py:395
  161.3 1.9 copy-done
  164.1 9.7 %shard_map.182 = (f32[768,256]{1,0:T(8,128)}, bf16[768,256]{1,0:T(8,128)(2,1)}, f32[2,128,128]{2,1,0:T(8,128)}, f32[2,1,128]{2,1,0:T(1,128)}) custom-call(bf16[768,2560]{1,0:T(8,128)(2,1)} %copy-done, bf16[768,2560]{1,0:T(8,128)(2,1)} %copy-done, bf16[768,2560]{1,0:T(8,128)(2,1)} %copy-done, f32[1,256]{1,0:T(1,128)} %bitcast.290, f32[768,256]{1,0:T(8,128)} %ds_ref.1), custom_call_target="tpu_custom_call" | custom-call | tf_op jit(solution)/shard_map/pallas_call | solution.py:327
  173.7 1.4 copy.76
  177.3 13.0 %shard_map.183 = (bf16[8,2,144,128]{3,2,1,0:T(8,128)(2,1)}, bf16[32,256]{1,0:T(8,128)(2,1)}) custom-call(bf16[2,144,128]{2,1,0:T(8,128)(2,1)} %pad_maximum_fusion.1.own, bf16[32,256]{1,0:T(8,128)(2,1)} %slice.469.rim), custom_call_target="tpu_custom_call" | custom-call | tf_op jit(solution)/shard_map/pallas_call | solution.py:243
  191.9 3.8 %multiply_reduce_fusion.1 = (f32[768]{0:T(1024)}, f32[768,256]{1,0:T(8,128)S(1)}) fusion(f32[798,256]{1,0:T(8,128)S(1)} %maximum_convert_fusion, f32[256]{0:T(256)S(1)} %bitcast.269, f32[256]{0:T(256)S(1)} %bitcast.270, f32[256]{0:T(256)S(1)} %bitcast.272, f32[256]{0:T(256)S(1)} %bitcast.273, f32[256]{0:T(256)S(1)} %bitcast.274, f32[256]{0:T(256)S(1)} %bitcast.275, ...), kind=kLoop, calls=%fused_computation.107 | loop fusion | flops 12385536 | bytes 25200640 | tf_op jit(solution)/shard_map/reduce_sum | solution.py:439
  195.8 5.2 %shard_map.184 = f32[4,6,128]{2,1,0:T(8,128)} custom-call(f32[6,128]{1,0:T(8,128)} %bitcast.251), custom_call_target="tpu_custom_call" | custom-call | tf_op jit(solution)/shard_map/pallas_call | solution.py:102
  202.8 1.5 multiply_convert_fusion
  204.4 1.8 slice_convert_fusion
  206.2 0.9 pad_maximum_fusion.own
  207.1 25.3 %shard_map.185 = bf16[4,768,512]{2,1,0:T(8,128)(2,1)} custom-call(bf16[768,512]{1,0:T(8,128)(2,1)} %pad_maximum_fusion.own), custom_call_target="tpu_custom_call" | custom-call | tf_op jit(solution)/shard_map/pallas_call | solution.py:102
  232.5 1.4 fusion.76
  233.9 1.4 convolution_add_fusion.8
  235.4 1.2 convolution_add_fusion.7
  240.0 1.8 fusion.16
  (69 shorter events, 14.4 us)
Async XLA Ops:
  0.0 8.8 %copy-start.10 = (bf16[256,256]{1,0:T(8,128)(2,1)S(1)}, bf16[256,256]{1,0:T(8,128)(2,1)}, u32[]{:S(2)}) copy-start(bf16[256,256]{1,0:T(8,128)(2,1)} %param.37) | copy-start | bytes 393220
  0.0 8.8 %copy-start.9 = (bf16[256,256]{1,0:T(8,128)(2,1)S(1)}, bf16[256,256]{1,0:T(8,128)(2,1)}, u32[]{:S(2)}) copy-start(bf16[256,256]{1,0:T(8,128)(2,1)} %param.36) | copy-start | bytes 393220
  0.0 8.7 %copy-start.8 = (bf16[256,512]{1,0:T(8,128)(2,1)S(1)}, bf16[256,512]{1,0:T(8,128)(2,1)}, u32[]{:S(2)}) copy-start(bf16[256,512]{1,0:T(8,128)(2,1)} %param.28) | copy-start | bytes 786436
  0.0 8.7 %copy-start.7 = (bf16[256,512]{1,0:T(8,128)(2,1)S(1)}, bf16[256,512]{1,0:T(8,128)(2,1)}, u32[]{:S(2)}) copy-start(bf16[256,512]{1,0:T(8,128)(2,1)} %param.27) | copy-start | bytes 786436
  8.8 1.2 copy-start.4
  144.6 4.8 %copy-start.2 = (bf16[4,192,2048]{2,1,0:T(8,128)(2,1)S(1)}, bf16[4,192,2048]{2,1,0:T(8,128)(2,1)}, u32[]{:S(2)}) copy-start(bf16[4,192,2048]{2,1,0:T(8,128)(2,1)} %get-tuple-element.14) | copy-start | bytes 9437188
  144.7 4.8 %copy-start.11 = (f32[2048]{0:T(1024)S(1)}, f32[2048]{0:T(1024)}, u32[]{:S(2)}) copy-start(f32[2048]{0:T(1024)} %param.20) | copy-start | bytes 24580
  161.3 1.9 copy-start
  191.9 9.8 %copy-start.5 = (bf16[8,2,144,128]{3,2,1,0:T(8,128)(2,1)S(1)}, bf16[8,2,144,128]{3,2,1,0:T(8,128)(2,1)}, u32[]{:S(2)}) copy-start(bf16[8,2,144,128]{3,2,1,0:T(8,128)(2,1)} %get-tuple-element.19) | copy-start | bytes 1769476
  191.9 9.9 %copy-start.6 = (bf16[768,256]{1,0:T(8,128)(2,1)S(1)}, bf16[768,256]{1,0:T(8,128)(2,1)}, u32[]{:S(2)}) copy-start(bf16[768,256]{1,0:T(8,128)(2,1)} %get-tuple-element.20) | copy-start | bytes 1179652
  195.8 6.4 %copy-start.14 = (f32[256]{0:T(256)S(1)}, f32[256]{0:T(256)}, u32[]{:S(2)}) copy-start(f32[256]{0:T(256)} %param.32) | copy-start | bytes 3076
  202.1 0.7 copy-start.12
  202.2 0.7 copy-start.13
  232.5 2.9 %copy-start.1 = (bf16[4,768,512]{2,1,0:T(8,128)(2,1)S(1)}, bf16[4,768,512]{2,1,0:T(8,128)(2,1)}, u32[]{:S(2)}) copy-start(bf16[4,768,512]{2,1,0:T(8,128)(2,1)} %shard_map.185) | copy-start | bytes 9437188
  233.9 2.6 %copy-start.3 = (bf16[4,2,256,512]{3,2,1,0:T(8,128)(2,1)S(1)}, bf16[4,2,256,512]{3,2,1,0:T(8,128)(2,1)}, u32[]{:S(2)}) copy-start(bf16[4,2,256,512]{3,2,1,0:T(8,128)(2,1)} %fusion.57) | copy-start | bytes 6291460

commit v3 on v2

--- a/solution.py
+++ b/solution.py
@@ -91,23 +91,30 @@
     pl.semaphore_wait(barrier, len(others) + 1 + len(extra))
 
 
-def tp_gather_kernel(m, own, out, send, recv, local_sem):
+def tp_gather_kernel(m, pieces, own, out, send, recv, local_sem):
     greet([], m)
-    state = tp_start(own, out, m, send, recv, local_sem)
-    tp_finish(tp_forward(own, out, m, send, recv, state))
-
-
-def tp_gather(block, cid):
+    size = own.shape[0] // pieces
+    views = []
+    for c in range(pieces):
+        rows = pl.ds(c * size, size)
+        views.append((own.at[rows], out.at[:, rows], m, send.at[c], recv.at[c]))
+    states = [tp_start(*view, local_sem.at[c]) for c, view in enumerate(views)]
+    states = [tp_forward(*view, state) for view, state in zip(views, states)]
+    for state in states:
+        tp_finish(state)
+
+
+def tp_gather(block, cid, pieces=1):
     m = lax.axis_size("tp")
     return pl.pallas_call(
-        functools.partial(tp_gather_kernel, m),
+        functools.partial(tp_gather_kernel, m, pieces),
         out_shape=jax.ShapeDtypeStruct((m,) + block.shape, block.dtype),
         in_specs=[pl.BlockSpec(memory_space=pl.ANY)],
         out_specs=pl.BlockSpec(memory_space=pl.ANY),
         scratch_shapes=[
-            pltpu.SemaphoreType.DMA((m,)),
-            pltpu.SemaphoreType.DMA((m,)),
-            pltpu.SemaphoreType.DMA,
+            pltpu.SemaphoreType.DMA((pieces, m)),
+            pltpu.SemaphoreType.DMA((pieces, m)),
+            pltpu.SemaphoreType.DMA((pieces,)),
         ],
         compiler_params=pltpu.CompilerParams(collective_id=cid, has_side_effects=True),
     )(block)
@@ -441,7 +448,7 @@
     scale = lax.rsqrt(squares / CONV + EPSILON)[:, None]
     mixed_conv = jax.nn.silu(conv_out * scale * channel_gain + channel_bias).astype(jnp.bfloat16)
 
-    both = tp_gather(jnp.concatenate([mixed_rec, mixed_conv], axis=1), 1)
+    both = tp_gather(jnp.concatenate([mixed_rec, mixed_conv], axis=1), 1, 3)
 
     def project(branch):
         first = branch * out_columns

time: 244 us -> 244 us (level)
  no operation moved by 1% of the time
where the time goes in v3:
time: 244 us; the launch traced here: 242 us
  Pallas kernels  188 us (77%)
  matrix products  18.8 us (8%)
  other arithmetic  17.5 us (7%)
  local copies, waits for them, and re-layouts  17.2 us (7%)
    pallas_call x1, Pallas kernels, ring_gather(): pl.pallas_call(functools.partial(ring_kernel, n, m, first), out_shape=(ja...  135 us
    pallas_call x2, Pallas kernels, tp_gather(): pl.pallas_call(functools.partial(tp_gather_kernel, m, pieces), out_shape=...  30.7 us
    pallas_call x1, Pallas kernels, exchange(): pl.pallas_call(functools.partial(exchange_kernel, n), out_shape=(jax.Shap...  13 us
    dot_general x1, matrix products, local(): jnp.dot(normed, stacked[:, :inputs_width], preferred_element_type=jnp.flo...  11.1 us
    unnamed x41, local copies, waits for them, and re-layouts  9.87 us
    pallas_call x1, Pallas kernels, recurrence(): pl.pallas_call(recurrence_kernel, grid=(heads,), out_shape=(jax.ShapeDtyp...  9.65 us
    dot_general x16, matrix products, project(): jnp.dot(both[t, :, branch * width:(branch + 1) * width], out_w[t, j, :, f...  7.42 us

profile of v3, /device:TPU:0, one launch (start us, length us, event | category | flops | bytes accessed | tf_op | source)
XLA Modules:
  0.0 242.0 jit_solution(2730902682708758872)
XLA Ops:
  0.0 1.1 fusion.129
  1.1 1.0 fusion.128
  2.1 1.0 copy.40
  5.0 0.9 constant_dynamic-update-slice_fusion.7
  5.9 0.9 constant_dynamic-update-slice_fusion.6
  8.8 1.2 copy-done.4
  10.0 134.6 %shard_map.181 = (bf16[8,256,3072]{2,1,0:T(8,128)(2,1)}, bf16[4,192,2048]{2,1,0:T(8,128)(2,1)}, bf16[4,2,256,512]{3,2,1,0:T(8,128)(2,1)}) custom-call(bf16[256,3072]{1,0:T(8,128)(2,1)} %copy-done.4, bf16[192,2048]{1,0:T(8,128)(2,1)} %tok.1), custom_call_target="tpu_custom_call" | custom-call | tf_op jit(solution)/shard_map/pallas_call | solution.py:271
  144.7 2.1 fusion.57
  146.7 2.6 %multiply_reduce_fusion = f32[4,192]{1,0:T(4,128)S(1)} fusion(bf16[4,192,2048]{2,1,0:T(8,128)(2,1)} %get-tuple-element.14), kind=kLoop, calls=%fused_computation.5 | loop fusion | flops 4717824 | bytes 3148800 | tf_op jit(solution)/shard_map/reduce_sum | solution.py:20
  150.2 11.1 %fusion.4.q_ref.f_ref.i_ref = bf16[768,2560]{1,0:T(8,128)(2,1)S(1)} fusion(bf16[768,2048]{1,0:T(8,128)(2,1)S(1)} %fusion.3, bf16[2048,3072]{1,0:T(8,128)(2,1)} %bitcast.250), kind=kOutput, calls=%fused_computation.6 | convolution fusion | flops 8055029760 | bytes 17563648 | tf_op jit(solution)/shard_map/dot_general | solution.py:402
  161.3 1.9 copy-done
  164.1 9.7 %shard_map.182 = (f32[768,256]{1,0:T(8,128)}, bf16[768,256]{1,0:T(8,128)(2,1)}, f32[2,128,128]{2,1,0:T(8,128)}, f32[2,1,128]{2,1,0:T(1,128)}) custom-call(bf16[768,2560]{1,0:T(8,128)(2,1)} %copy-done, bf16[768,2560]{1,0:T(8,128)(2,1)} %copy-done, bf16[768,2560]{1,0:T(8,128)(2,1)} %copy-done, f32[1,256]{1,0:T(1,128)} %bitcast.290, f32[768,256]{1,0:T(8,128)} %ds_ref.1), custom_call_target="tpu_custom_call" | custom-call | tf_op jit(solution)/shard_map/pallas_call | solution.py:334
  173.7 1.4 copy.76
  177.3 13.0 %shard_map.183 = (bf16[8,2,144,128]{3,2,1,0:T(8,128)(2,1)}, bf16[32,256]{1,0:T(8,128)(2,1)}) custom-call(bf16[2,144,128]{2,1,0:T(8,128)(2,1)} %pad_maximum_fusion.1.own, bf16[32,256]{1,0:T(8,128)(2,1)} %slice.469.rim), custom_call_target="tpu_custom_call" | custom-call | tf_op jit(solution)/shard_map/pallas_call | solution.py:250
  191.9 3.8 %multiply_reduce_fusion.1 = (f32[768]{0:T(1024)}, f32[768,256]{1,0:T(8,128)S(1)}) fusion(f32[798,256]{1,0:T(8,128)S(1)} %maximum_convert_fusion, f32[256]{0:T(256)S(1)} %bitcast.269, f32[256]{0:T(256)S(1)} %bitcast.270, f32[256]{0:T(256)S(1)} %bitcast.272, f32[256]{0:T(256)S(1)} %bitcast.273, f32[256]{0:T(256)S(1)} %bitcast.274, f32[256]{0:T(256)S(1)} %bitcast.275, ...), kind=kLoop, calls=%fused_computation.107 | loop fusion | flops 12385536 | bytes 25200640 | tf_op jit(solution)/shard_map/reduce_sum | solution.py:446
  195.8 5.2 %shard_map.184 = f32[4,6,128]{2,1,0:T(8,128)} custom-call(f32[6,128]{1,0:T(8,128)} %bitcast.251), custom_call_target="tpu_custom_call" | custom-call | tf_op jit(solution)/shard_map/pallas_call | solution.py:109
  202.8 1.5 multiply_convert_fusion
  204.4 1.8 slice_convert_fusion
  206.2 0.9 pad_maximum_fusion.own
  207.1 25.5 %shard_map.185 = bf16[4,768,512]{2,1,0:T(8,128)(2,1)} custom-call(bf16[768,512]{1,0:T(8,128)(2,1)} %pad_maximum_fusion.own), custom_call_target="tpu_custom_call" | custom-call | tf_op jit(solution)/shard_map/pallas_call | solution.py:109
  232.6 1.4 fusion.76
  234.1 1.4 convolution_add_fusion.8
  235.5 1.2 convolution_add_fusion.7
  240.2 1.8 fusion.16
  (69 shorter events, 14.4 us)
Async XLA Ops:
  0.0 8.8 %copy-start.10 = (bf16[256,256]{1,0:T(8,128)(2,1)S(1)}, bf16[256,256]{1,0:T(8,128)(2,1)}, u32[]{:S(2)}) copy-start(bf16[256,256]{1,0:T(8,128)(2,1)} %param.37) | copy-start | bytes 393220
  0.0 8.8 %copy-start.9 = (bf16[256,256]{1,0:T(8,128)(2,1)S(1)}, bf16[256,256]{1,0:T(8,128)(2,1)}, u32[]{:S(2)}) copy-start(bf16[256,256]{1,0:T(8,128)(2,1)} %param.36) | copy-start | bytes 393220
  0.0 8.7 %copy-start.8 = (bf16[256,512]{1,0:T(8,128)(2,1)S(1)}, bf16[256,512]{1,0:T(8,128)(2,1)}, u32[]{:S(2)}) copy-start(bf16[256,512]{1,0:T(8,128)(2,1)} %param.28) | copy-start | bytes 786436
  0.0 8.7 %copy-start.7 = (bf16[256,512]{1,0:T(8,128)(2,1)S(1)}, bf16[256,512]{1,0:T(8,128)(2,1)}, u32[]{:S(2)}) copy-start(bf16[256,512]{1,0:T(8,128)(2,1)} %param.27) | copy-start | bytes 786436
  8.8 1.2 copy-start.4
  144.6 4.8 %copy-start.2 = (bf16[4,192,2048]{2,1,0:T(8,128)(2,1)S(1)}, bf16[4,192,2048]{2,1,0:T(8,128)(2,1)}, u32[]{:S(2)}) copy-start(bf16[4,192,2048]{2,1,0:T(8,128)(2,1)} %get-tuple-element.14) | copy-start | bytes 9437188
  144.7 4.8 %copy-start.11 = (f32[2048]{0:T(1024)S(1)}, f32[2048]{0:T(1024)}, u32[]{:S(2)}) copy-start(f32[2048]{0:T(1024)} %param.20) | copy-start | bytes 24580
  161.3 1.9 copy-start
  191.9 9.8 %copy-start.5 = (bf16[8,2,144,128]{3,2,1,0:T(8,128)(2,1)S(1)}, bf16[8,2,144,128]{3,2,1,0:T(8,128)(2,1)}, u32[]{:S(2)}) copy-start(bf16[8,2,144,128]{3,2,1,0:T(8,128)(2,1)} %get-tuple-element.19) | copy-start | bytes 1769476
  191.9 9.9 %copy-start.6 = (bf16[768,256]{1,0:T(8,128)(2,1)S(1)}, bf16[768,256]{1,0:T(8,128)(2,1)}, u32[]{:S(2)}) copy-start(bf16[768,256]{1,0:T(8,128)(2,1)} %get-tuple-element.20) | copy-start | bytes 1179652
  195.8 6.4 %copy-start.14 = (f32[256]{0:T(256)S(1)}, f32[256]{0:T(256)}, u32[]{:S(2)}) copy-start(f32[256]{0:T(256)} %param.32) | copy-start | bytes 3076
  202.1 0.7 copy-start.12
  202.2 0.7 copy-start.13
  232.6 2.9 %copy-start.1 = (bf16[4,768,512]{2,1,0:T(8,128)(2,1)S(1)}, bf16[4,768,512]{2,1,0:T(8,128)(2,1)}, u32[]{:S(2)}) copy-start(bf16[4,768,512]{2,1,0:T(8,128)(2,1)} %shard_map.185) | copy-start | bytes 9437188
  234.1 2.6 %copy-start.3 = (bf16[4,2,256,512]{3,2,1,0:T(8,128)(2,1)S(1)}, bf16[4,2,256,512]{3,2,1,0:T(8,128)(2,1)}, u32[]{:S(2)}) copy-start(bf16[4,2,256,512]{3,2,1,0:T(8,128)(2,1)} %fusion.57) | copy-start | bytes 6291460
